TPU v7x, 32 devices: a whole 2x2x4 slice. The times are simulated.
32 devices in a mesh: sp: 4 (over z), tp: 8 (over y, x, core).
Axes of the slice: x: 2, y: 2, z: 4, core: 2. Of those that a mesh axis runs over, the one named last changes fastest.
Arguments:
- target_rows: bfloat16 [768, 2048], P(('sp', 'tp')), may hold values from -6 to 6
- source_rows: bfloat16 [4096, 2048], P(('sp', 'tp')), may hold values from -6 to 6
- target_gain: float32 [2048], replicated, may hold values from 0.55 to 9
- source_gain: float32 [2048], replicated, may hold values from 0.55 to 9
- query_weight: bfloat16 [2048, 2048], P(None, 'tp'), may hold values from -0.125 to 0.125
- key_weight: bfloat16 [2048, 512], P('tp'), may hold values from -0.125 to 0.125
- value_weight: bfloat16 [2048, 512], P('tp'), may hold values from -0.125 to 0.125
- out_weight: bfloat16 [2048, 2048], P('tp'), may hold values from -0.125 to 0.125
- out_cotangent: bfloat16 [768, 2048], P(('sp', 'tp')), may hold values from -6 to 6
Outputs:
- target_grad: float32 [768, 2048], P(('sp', 'tp'))
- source_grad: float32 [4096, 2048], P(('sp', 'tp'))
- out_weight_grad: float32 [2048, 2048], P('tp')
All inputs are finite; a program needn't handle non-finite values.
Results may differ from a plain program's by a relative error of at most 0.03.
Values may be sent and summed in bfloat16 or wider, within the bound.
A program may use at most 64 MiB of HBM per device.

v0:
```python
import jax
import jax.numpy as jnp
from jax import lax
from jax.sharding import PartitionSpec as P

HEAD_DIM = 64
KV_HEADS = 8
EPSILON = 1e-06
NEGATIVE = -1e30


def normalize(matrix, gain_vector):
    widened = matrix.astype(jnp.float32)
    factor = lax.rsqrt(jnp.mean(widened * widened, axis=-1, keepdims=True) + EPSILON)
    return (widened * factor * gain_vector).astype(jnp.bfloat16)


def norm_back(matrix, gain_vector, upstream):
    widened = matrix.astype(jnp.float32)
    factor = lax.rsqrt(jnp.mean(widened * widened, axis=-1, keepdims=True) + EPSILON)
    weighted = upstream * gain_vector
    inner_sum = jnp.mean(weighted * widened, axis=-1, keepdims=True)
    return factor * weighted - widened * factor**3 * inner_sum


def block_rows_for(length):
    return 512 if length % 512 == 0 else length


def body(
    target_rows,
    source_rows,
    target_gain,
    source_gain,
    query_weight,
    key_weight,
    value_weight,
    out_weight,
    out_cotangent,
):
    tp_count = lax.axis_size("tp")
    local_heads = query_weight.shape[1] // HEAD_DIM
    slot_heads = max(1, KV_HEADS // tp_count)
    copies = max(1, tp_count // KV_HEADS)
    per_slot = local_heads // slot_heads
    score_scale = HEAD_DIM ** (-0.5)
    normed_t = normalize(target_rows, target_gain)
    normed_s = normalize(source_rows, source_gain)
    source_local = normed_s.shape[0]
    key_full, value_full = (
        lax.all_gather(key_weight, "tp", axis=0, tiled=True),
        lax.all_gather(value_weight, "tp", axis=0, tiled=True),
    )
    key_own = jnp.dot(normed_s, key_full, preferred_element_type=jnp.float32).astype(jnp.bfloat16)
    value_own = jnp.dot(normed_s, value_full, preferred_element_type=jnp.float32).astype(
        jnp.bfloat16
    )

    def to_slots(matrix):
        split_heads = matrix.reshape(source_local, KV_HEADS, 1, HEAD_DIM)
        spread = jnp.broadcast_to(split_heads, (source_local, KV_HEADS, copies, HEAD_DIM))
        return spread.reshape(source_local, tp_count, slot_heads * HEAD_DIM)

    key_slots, value_slots = (
        lax.all_to_all(to_slots(key_own), "tp", split_axis=1, concat_axis=0, tiled=True),
        lax.all_to_all(to_slots(value_own), "tp", split_axis=1, concat_axis=0, tiled=True),
    )
    source_block = key_slots.shape[0]
    key_flat = key_slots.reshape(source_block, slot_heads * HEAD_DIM)
    value_flat = value_slots.reshape(source_block, slot_heads * HEAD_DIM)
    pieces = lax.all_gather((normed_t, out_cotangent), "tp", axis=0, tiled=True)
    queries = jnp.dot(pieces[0], query_weight, preferred_element_type=jnp.float32).astype(
        jnp.bfloat16
    )
    d_attended = jnp.dot(pieces[1], out_weight.T, preferred_element_type=jnp.float32).astype(
        jnp.bfloat16
    )
    queries, d_attended, cotangent_block = (queries, d_attended, pieces[1])
    target_block = queries.shape[0]
    query_view = queries.reshape(target_block, slot_heads, per_slot, HEAD_DIM)
    start_state = (
        jnp.full((slot_heads, per_slot, target_block), NEGATIVE, jnp.float32),
        jnp.zeros((slot_heads, per_slot, target_block), jnp.float32),
        jnp.zeros((slot_heads, per_slot, target_block, HEAD_DIM), jnp.float32),
    )
    running = start_state
    pieces = (
        lax.all_gather(key_flat, "sp", axis=0, tiled=True),
        lax.all_gather(value_flat, "sp", axis=0, tiled=True),
    )
    length = pieces[0].shape[0]
    step_rows = 2048

    def one_block(carried, block_index):
        prior_max, prior_total, prior_sum = carried
        key_part = lax.dynamic_slice_in_dim(pieces[0], block_index * step_rows, step_rows, 0)
        value_part = lax.dynamic_slice_in_dim(pieces[1], block_index * step_rows, step_rows, 0)
        key_part = key_part.reshape(step_rows, slot_heads, HEAD_DIM)
        value_part = value_part.reshape(step_rows, slot_heads, HEAD_DIM)
        scores = (
            jnp.einsum("tgqd,sgd->gqts", query_view, key_part, preferred_element_type=jnp.float32)
            * score_scale
        )
        new_max = jnp.maximum(prior_max, jnp.max(scores, axis=-1))
        rescale = jnp.exp(prior_max - new_max)
        weights = jnp.exp(scores - new_max[..., None])
        new_total = prior_total * rescale + jnp.sum(weights, axis=-1)
        new_sum = prior_sum * rescale[..., None] + jnp.einsum(
            "gqts,sgd->gqtd",
            weights.astype(jnp.bfloat16),
            value_part,
            preferred_element_type=jnp.float32,
        )
        return ((new_max, new_total, new_sum), None)

    running, unused = lax.scan(one_block, running, jnp.arange(length // step_rows))
    row_max, total, summed = running
    attended = (
        (summed / total[..., None])
        .transpose(2, 0, 1, 3)
        .reshape(target_block, local_heads * HEAD_DIM)
        .astype(jnp.bfloat16)
    )
    log_total = (row_max + jnp.log(total)).transpose(2, 0, 1).reshape(target_block, local_heads)
    delta = jnp.sum(
        (d_attended.astype(jnp.float32) * attended.astype(jnp.float32)).reshape(
            target_block, local_heads, HEAD_DIM
        ),
        axis=-1,
    )
    all_queries, all_grads = (
        lax.all_gather(queries, "sp", axis=0, tiled=True),
        lax.all_gather(d_attended, "sp", axis=0, tiled=True),
    )
    all_logs, all_deltas = (
        lax.all_gather(log_total, "sp", axis=0, tiled=True),
        lax.all_gather(delta, "sp", axis=0, tiled=True),
    )
    whole_rows = all_queries.shape[0]
    step_rows = block_rows_for(whole_rows)
    block_shape = (whole_rows // step_rows, step_rows, slot_heads, per_slot)
    query_blocks = all_queries.reshape(block_shape + (HEAD_DIM,))
    grad_blocks = all_grads.reshape(block_shape + (HEAD_DIM,))
    log_blocks = all_logs.reshape(block_shape)
    delta_blocks = all_deltas.reshape(block_shape)

    def backward_block(sums_so_far, inputs):
        key_sum, value_sum = sums_so_far
        query_part, grad_part, log_part, delta_part = inputs
        scores = (
            jnp.einsum("tgqd,sgd->gqts", query_part, key_slots, preferred_element_type=jnp.float32)
            * score_scale
        )
        probs = jnp.exp(scores - log_part.transpose(1, 2, 0)[..., None])
        value_sum = value_sum + jnp.einsum(
            "gqts,tgqd->sgd",
            probs.astype(jnp.bfloat16),
            grad_part,
            preferred_element_type=jnp.float32,
        )
        d_probs = jnp.einsum(
            "tgqd,sgd->gqts", grad_part, value_slots, preferred_element_type=jnp.float32
        )
        d_scores = (probs * (d_probs - delta_part.transpose(1, 2, 0)[..., None])).astype(
            jnp.bfloat16
        )
        d_query = (
            jnp.einsum("gqts,sgd->tgqd", d_scores, key_slots, preferred_element_type=jnp.float32)
            * score_scale
        )
        key_sum = (
            key_sum
            + jnp.einsum("gqts,tgqd->sgd", d_scores, query_part, preferred_element_type=jnp.float32)
            * score_scale
        )
        return ((key_sum, value_sum), d_query)

    zero_sums = jnp.zeros((source_block, slot_heads, HEAD_DIM), jnp.float32)
    (key_sum, value_sum), d_query = lax.scan(
        backward_block,
        (zero_sums, zero_sums),
        (query_blocks, grad_blocks, log_blocks, delta_blocks),
    )
    query_terms = d_query.reshape(whole_rows, local_heads * HEAD_DIM)
    query_grad = lax.psum_scatter(query_terms, "sp", scatter_dimension=0, tiled=True).astype(
        jnp.bfloat16
    )
    key_back, value_back = (
        lax.all_to_all(key_sum, "tp", split_axis=0, concat_axis=1, tiled=True),
        lax.all_to_all(value_sum, "tp", split_axis=0, concat_axis=1, tiled=True),
    )

    def from_slots(matrix):
        folded = jnp.sum(matrix.reshape(source_local, KV_HEADS, copies, HEAD_DIM), axis=2)
        return folded.reshape(source_local, KV_HEADS * HEAD_DIM).astype(jnp.bfloat16)

    key_grad = from_slots(key_back)
    value_grad = from_slots(value_back)
    d_normed_s = jnp.dot(key_grad, key_full.T, preferred_element_type=jnp.float32) + jnp.dot(
        value_grad, value_full.T, preferred_element_type=jnp.float32
    )
    source_grad = norm_back(source_rows, source_gain, d_normed_s)
    d_normed_t = lax.psum_scatter(
        jnp.dot(query_grad, query_weight.T, preferred_element_type=jnp.float32),
        "tp",
        scatter_dimension=0,
        tiled=True,
    )
    target_grad = out_cotangent.astype(jnp.float32) + norm_back(
        target_rows, target_gain, d_normed_t
    )
    weight_part = jnp.dot(attended.T, cotangent_block, preferred_element_type=jnp.float32)
    out_weight_grad = lax.psum(weight_part, "sp")
    return (target_grad, source_grad, out_weight_grad)


def solution(mesh):
    return jax.shard_map(
        body,
        mesh=mesh,
        in_specs=(
            P(("sp", "tp"), None),
            P(("sp", "tp"), None),
            P(),
            P(),
            P(None, "tp"),
            P("tp", None),
            P("tp", None),
            P("tp", None),
            P(("sp", "tp"), None),
        ),
        out_specs=(P(("sp", "tp"), None), P(("sp", "tp"), None), P("tp", None)),
        check_vma=False,
    )
```

profile of v0, /device:TPU:0, one launch (start us, length us, event | category | flops | bytes accessed | tf_op | source)
XLA Modules:
  0.0 356.4 jit_solution(7738776949373914293)
XLA Ops:
  7.2 0.7 all-gather.5.cloned.1.call-update
  8.0 0.7 all-gather.7.cloned.1.call-update
  8.7 1.0 fusion.42
  9.7 0.6 multiply_multiply_fusion.1
  10.3 1.0 fusion.44
  11.3 11.9 %all_gather.31 = bf16[192,2048]{1,0:T(8,128)(2,1)S(1)} all-gather(bf16[24,2048]{1,0:T(8,128)(2,1)S(1)} %fusion.44), channel_id=1, replica_groups=mesh['sp'=4,'tp'=8] {'tp'}, dimensions={0}, use_global_device_ids=true | all-gather | bytes 884736 | tf_op jit(solution)/shard_map/all_gather | solution.py:71
  23.2 0.4 convolution_convert_fusion.3
  23.5 0.8 copy.77
  24.3 15.0 %all_gather.32 = bf16[768,256]{1,0:T(8,128)(2,1)S(1)} all-gather(bf16[192,256]{1,0:T(8,128)(2,1)S(1)} %convolution_convert_fusion.3), channel_id=1, replica_groups=mesh['sp'=4,'tp'=8] {'sp'}, dimensions={0}, use_global_device_ids=true | all-gather | bytes 491520 | tf_op jit(solution)/shard_map/all_gather | solution.py:132
  39.5 1.2 fusion.36
  40.7 11.7 %all_gather.37 = bf16[192,2048]{1,0:T(8,128)(2,1)S(1)} all-gather(bf16[24,2048]{1,0:T(8,128)(2,1)} %param.19), channel_id=1, replica_groups=mesh['sp'=4,'tp'=8] {'tp'}, dimensions={0}, use_global_device_ids=true | all-gather | bytes 884736 | tf_op jit(solution)/shard_map/all_gather | solution.py:71
  52.4 0.6 multiply_multiply_fusion
  53.0 2.1 convolution_convert_fusion.1
  55.1 0.8 copy.74
  55.8 3.4 all-to-all-start
  59.2 11.9 %all-gather.7.cloned.1.call-done = bf16[2048,512]{1,0:T(8,128)(2,1)} async-done(((bf16[256,512]{1,0:T(8,128)(2,1)}), bf16[2048,512]{1,0:T(8,128)(2,1)}) %all-gather.7.cloned.1.call-update) | async-done | bytes 2097168 | tf_op jit(solution)/shard_map/all_gather | solution.py:52
  71.2 2.1 convolution_convert_fusion
  73.2 0.8 copy.78
  74.0 3.4 all-to-all-start.1
  77.5 0.7 reshape.179
  78.3 16.4 %all_gather.33 = bf16[4096,64]{0,1:T(8,128)(2,1)S(1)} all-gather(bf16[1024,64]{0,1:T(8,128)(2,1)S(1)} %bitcast.239), channel_id=1, replica_groups=mesh['sp'=4,'tp'=8] {'sp'}, dimensions={0}, use_global_device_ids=true | all-gather | bytes 655360 | tf_op jit(solution)/shard_map/all_gather | solution.py:88
  94.8 0.7 reshape.180
  95.6 16.0 %all_gather.35 = bf16[4096,64]{0,1:T(8,128)(2,1)S(1)} all-gather(bf16[1024,64]{0,1:T(8,128)(2,1)S(1)} %bitcast.240), channel_id=1, replica_groups=mesh['sp'=4,'tp'=8] {'sp'}, dimensions={0}, use_global_device_ids=true | all-gather | bytes 655360 | tf_op jit(solution)/shard_map/all_gather | solution.py:89
  111.6 23.4 %while.3 = (s32[]{:T(128)}, f32[1,4,192]{2,1,0:T(4,128)S(1)}, f32[1,4,192]{2,1,0:T(4,128)S(1)}, f32[1,4,192,64]{2,3,1,0:T(8,128)S(1)}, s32[2]{0:T(128)S(1)}, /*i...) while((s32[]{:T(128)}, f32[1,4,192]{2,1,0:T(4,128)S(1)}, ...), condition=%wide.region_5.6_spmd.clone, body=%wide.region_2.5_spmd.clone.sunk | while | flops 415388160 | bytes 45173076 | solution.py:116
  111.6 0.6 dynamic_slice.38
  112.9 4.6 %bitcast_reduce_fusion.3 = (f32[4,192]{1,0:T(4,128)S(1)}, f32[2048,192,4]{0,1,2:T(8,128)}) fusion(bf16[192,1,4,64]{0,3,2,1:T(8,128)(2,1)} %get-tuple-element.230, bf16[4096,64]{0,1:T(8,128)(2,1)S(1)} %get-tuple-element.229, s32[]{:T(128)S(6)} %select_n.6), kind=kOutput, calls=%fused_computation.1.clone.1 | convolution fusion | flops 204471552 | bytes 6654980 | tf_op jit(solution)/shard_map/while/body/eval_jaxpr/tgqd,sgd->gqts/dot_general | solution.py:101
  117.5 4.3 %fusion.90 = f32[1,4,192,64]{2,3,1,0:T(8,128)S(1)} fusion(f32[2048,192,4]{0,1,2:T(8,128)} %get-tuple-element.198, f32[4,192]{1,0:T(4,128)S(1)} %bitcast.230, f32[1,4,192,64]{2,3,1,0:T(8,128)S(1)} %get-tuple-element.215, bf16[4096,64]{0,1:T(8,128)(2,1)S(1)} %get-tuple-element.231, s32[]{:T(128)S(6)} %select_n.6, f32[4,192]{1,0:T(4,128)S(1)} %get-tuple-element.199, ...), kind=kOutput, calls=%fused_computation.8.clone.1 | convolution fusion | flops 206192640 | bytes 7020549 | tf_op jit(solution)/shard_map/while/body/eval_jaxpr/gqts,sgd->gqtd/dot_general | solution.py:108
  122.1 1.2 fusion.89
  123.3 0.7 dynamic_slice.38
  124.6 4.6 %bitcast_reduce_fusion.3 = (f32[4,192]{1,0:T(4,128)S(1)}, f32[2048,192,4]{0,1,2:T(8,128)}) fusion(bf16[192,1,4,64]{0,3,2,1:T(8,128)(2,1)} %get-tuple-element.230, bf16[4096,64]{0,1:T(8,128)(2,1)S(1)} %get-tuple-element.229, s32[]{:T(128)S(6)} %select_n.6), kind=kOutput, calls=%fused_computation.1.clone.1 | convolution fusion | flops 204471552 | bytes 6654980 | tf_op jit(solution)/shard_map/while/body/eval_jaxpr/tgqd,sgd->gqts/dot_general | solution.py:101
  129.2 4.3 %fusion.90 = f32[1,4,192,64]{2,3,1,0:T(8,128)S(1)} fusion(f32[2048,192,4]{0,1,2:T(8,128)} %get-tuple-element.198, f32[4,192]{1,0:T(4,128)S(1)} %bitcast.230, f32[1,4,192,64]{2,3,1,0:T(8,128)S(1)} %get-tuple-element.215, bf16[4096,64]{0,1:T(8,128)(2,1)S(1)} %get-tuple-element.231, s32[]{:T(128)S(6)} %select_n.6, f32[4,192]{1,0:T(4,128)S(1)} %get-tuple-element.199, ...), kind=kOutput, calls=%fused_computation.8.clone.1 | convolution fusion | flops 206192640 | bytes 7020549 | tf_op jit(solution)/shard_map/while/body/eval_jaxpr/gqts,sgd->gqtd/dot_general | solution.py:108
  133.8 1.2 fusion.89
  135.1 1.7 convert_multiply_fusion.8
  136.9 15.1 %all_gather.38 = bf16[768,256]{1,0:T(8,128)(2,1)S(1)} all-gather(bf16[192,256]{1,0:T(8,128)(2,1)S(1)} %get-tuple-element.140), channel_id=1, replica_groups=mesh['sp'=4,'tp'=8] {'sp'}, dimensions={0}, use_global_device_ids=true | all-gather | bytes 491520 | tf_op jit(solution)/shard_map/all_gather | solution.py:133
  152.3 13.2 %all-gather.1 = f32[4,192,4]{1,2,0:T(4,128)S(1)} all-gather(f32[1,192,4]{1,2,0:T(4,128)S(1)} %bitcast.250), channel_id=1, replica_groups=mesh['sp'=4,'tp'=8] {'sp'}, dimensions={0}, use_global_device_ids=true | all-gather | bytes 15360 | tf_op jit(solution)/shard_map/all_gather | solution.py:137
  165.8 14.5 %all-gather = f32[768,1,4]{2,1,0:T(1,128)S(1)} all-gather(f32[192,1,4]{2,1,0:T(1,128)S(1)} %bitcast.247), channel_id=2, replica_groups=mesh['sp'=4,'tp'=8] {'sp'}, dimensions={0}, use_global_device_ids=true | all-gather | bytes 15360 | tf_op jit(solution)/shard_map/all_gather | solution.py:136
  180.5 2.8 fusion.54
  183.3 3.2 fusion.27
  186.5 1.3 copy-done.2
  187.8 1.2 convolution_multiply_fusion
  189.0 1.4 copy-done.3
  190.4 1.1 copy.98
  191.6 23.7 %reduce-scatter.7.cloned.1.call-done = f32[192,256]{1,0:T(8,128)} async-done(((f32[768,256]{1,0:T(8,128)}), f32[192,256]{1,0:T(8,128)}) %reduce-scatter.7.cloned.1.call-update) | async-done | bytes 196624
  215.3 1.0 copy.99
  216.3 1.7 fusion.57
  218.0 4.8 %fusion.35 = bf16[1024,1,64]{0,2,1:T(8,128)(2,1)S(1)} fusion(bf16[768,4,64]{0,2,1:T(8,128)(2,1)S(1)} %bitcast.225, bf16[4,768,1024]{1,2,0:T(8,128)(2,1)} %copy-done.3), kind=kOutput, calls=%fused_computation.43 | convolution fusion | flops 402784256 | bytes 6815744 | tf_op jit(solution)/shard_map/while/body/eval_jaxpr/gqts,tgqd->sgd/dot_general | solution.py:173
  222.8 0.5 broadcast.163
  223.3 0.7 reduce.2
  224.2 0.9 reshape.187
  225.1 3.6 %all-to-all-start.2 = ((bf16[8,2,4096]{2,1,0:T(2,128)(2,1)}), bf16[8,2,4096]{2,1,0:T(2,128)(2,1)S(1)}, u32[]{:S(2)}, u32[]{:S(2)}) async-start(bf16[8,2,4096]{2,1,0:T(2,128)(2,1)} %reshape.187), calls=%async_computation.3 | async-start | bytes 262144 | tf_op jit(solution)/shard_map/all_to_all | solution.py:189
  228.7 6.9 %fusion.31 = bf16[1024,1,64]{0,2,1:T(8,128)(2,1)S(1)} fusion(bf16[768,4,64]{0,2,1:T(8,128)(2,1)S(1)} %bitcast.228, f32[1024,768,4]{1,0,2:T(8,128)} %copy-done.2, f32[4,768]{1,0:T(4,128)S(1)} %copy.81), kind=kOutput, calls=%fused_computation.40 | convolution fusion | flops 412090368 | bytes 13119488 | tf_op jit(solution)/shard_map/while/body/eval_jaxpr/gqts,tgqd->sgd/dot_general | solution.py:155
  235.6 0.7 reduce.3
  236.5 0.9 reshape.189
  237.4 4.2 %all-to-all-start.3 = ((bf16[8,2,4096]{2,1,0:T(2,128)(2,1)}), bf16[8,2,4096]{2,1,0:T(2,128)(2,1)S(1)}, u32[]{:S(2)}, u32[]{:S(2)}) async-start(bf16[8,2,4096]{2,1,0:T(2,128)(2,1)} %reshape.189), calls=%async_computation.4 | async-start | bytes 262144 | tf_op jit(solution)/shard_map/all_to_all | solution.py:190
  241.6 1.8 fusion.56
  244.2 2.9 all-to-all-done.3
  247.8 2.4 fusion.55
  250.2 2.5 fusion.41
  252.8 1.3 fusion.40
  254.1 3.6 %reduce-scatter.5.cloned.1.call-done = f32[24,2048]{1,0:T(8,128)} async-done(((f32[192,2048]{1,0:T(8,128)}), f32[24,2048]{1,0:T(8,128)}) %reduce-scatter.5.cloned.1.call-update) | async-done | bytes 196624 | tf_op jit(solution)/shard_map/reduce_scatter | solution.py:203
  257.7 1.1 fusion.48
  258.8 1.7 fusion.47
  260.5 86.2 %all-reduce.2.cloned.1.call-done = f32[256,2048]{1,0:T(8,128)} async-done(((f32[256,2048]{1,0:T(8,128)}), f32[256,2048]{1,0:T(8,128)}) %all-reduce.2.cloned.1.call-update) | async-done | bytes 2097168 | tf_op jit(solution)/shard_map/psum | solution.py:213
  346.7 3.1 copy.123
  (91 shorter events, 3.9 us)
Async XLA Ops:
  7.2 16.0 %copy-start = (bf16[2048,256]{1,0:T(8,128)(2,1)S(1)}, bf16[2048,256]{1,0:T(8,128)(2,1)}, u32[]{:S(2)}) copy-start(bf16[2048,256]{1,0:T(8,128)(2,1)} %param.15) | copy-start | bytes 3145732
  7.2 45.8 %copy-start.4 = (bf16[128,2048]{1,0:T(8,128)(2,1)S(1)}, bf16[128,2048]{1,0:T(8,128)(2,1)}, u32[]{:S(2)}) copy-start(bf16[128,2048]{1,0:T(8,128)(2,1)} %param.12) | copy-start | bytes 1572868
  7.2 45.8 %copy-start.11 = (f32[2048]{0:T(1024)S(1)}, f32[2048]{0:T(1024)}, u32[]{:S(2)}) copy-start(f32[2048]{0:T(1024)} %param.14) | copy-start | bytes 24580
  7.2 45.8 %all-gather.5.cloned.1.call-start = ((), (), s32[]{:S(2)}) async-start(), calls=%async_computation.6 | async-start | bytes 2359296 | tf_op jit(solution)/shard_map/all_gather | solution.py:51
  7.9 63.2 %all-gather.7.cloned.1.call-start = ((), (), s32[]{:S(2)}) async-start(), calls=%async_computation.7 | async-start | bytes 2359296 | tf_op jit(solution)/shard_map/all_gather | solution.py:52
  53.0 42.6 %copy-start.15 = (f32[128]{0:T(128)}, f32[128]{0:T(128)S(1)}, u32[]{:S(2)}) copy-start(f32[128]{0:T(128)S(1)} %get-tuple-element.136) | copy-start | bytes 1540
  55.8 18.2 %all-to-all-start = ((bf16[128,8,64]{0,2,1:T(8,128)(2,1)}), bf16[128,8,64]{0,2,1:T(8,128)(2,1)S(1)}, u32[]{:S(2)}, u32[]{:S(2)}) async-start(bf16[128,8,64]{0,2,1:T(8,128)(2,1)} %bitcast), calls=%async_computation | async-start | bytes 262144 | tf_op jit(solution)/shard_map/all_to_all | solution.py:65
  74.0 20.7 %all-to-all-start.1 = ((bf16[128,8,64]{0,2,1:T(8,128)(2,1)}), bf16[128,8,64]{0,2,1:T(8,128)(2,1)S(1)}, u32[]{:S(2)}, u32[]{:S(2)}) async-start(bf16[128,8,64]{0,2,1:T(8,128)(2,1)} %bitcast.7), calls=%async_computation.1 | async-start | bytes 262144 | tf_op jit(solution)/shard_map/all_to_all | solution.py:66
  77.4 137.9 %reduce-scatter.7.cloned.1.call-start = ((), (), s32[]{:S(2)}) async-start(), calls=%async_computation.10 | async-start | bytes 983040
  111.6 1.3 copy-start.17
  117.5 4.6 %copy-start.1 = (f32[2048,192,4]{0,1,2:T(8,128)S(1)}, f32[2048,192,4]{0,1,2:T(8,128)}, u32[]{:S(2)}) copy-start(f32[2048,192,4]{0,1,2:T(8,128)} %get-tuple-element.198) | copy-start | bytes 18874372 | tf_op jit(solution)/shard_map/while
  117.5 5.8 %copy-start.18 = (s32[2]{0:T(128)S(1)}, s32[2]{0:T(128)}, u32[]{:S(2)}) copy-start(s32[2]{0:T(128)} %copy-done.17) | copy-start | bytes 28 | tf_op jit(solution)/shard_map/while
  123.3 1.3 copy-start.17
  129.2 4.6 %copy-start.1 = (f32[2048,192,4]{0,1,2:T(8,128)S(1)}, f32[2048,192,4]{0,1,2:T(8,128)}, u32[]{:S(2)}) copy-start(f32[2048,192,4]{0,1,2:T(8,128)} %get-tuple-element.198) | copy-start | bytes 18874372 | tf_op jit(solution)/shard_map/while
  129.2 5.8 %copy-start.18 = (s32[2]{0:T(128)S(1)}, s32[2]{0:T(128)}, u32[]{:S(2)}) copy-start(s32[2]{0:T(128)} %copy-done.17) | copy-start | bytes 28 | tf_op jit(solution)/shard_map/while
  180.5 2.8 copy-start.8
  183.3 4.5 %copy-start.2 = (f32[1024,768,4]{1,0,2:T(8,128)}, f32[1024,768,4]{1,0,2:T(8,128)S(1)}, u32[]{:S(2)}) copy-start(f32[1024,768,4]{1,0,2:T(8,128)S(1)} %fusion.54) | copy-start | bytes 37748740
  183.3 4.5 %copy-start.7 = (bf16[1024,64,1]{0,1,2:T(8,128)(2,1)S(1)}, bf16[1024,64,1]{0,1,2:T(8,128)(2,1)}, u32[]{:S(2)}) copy-start(bf16[1024,64,1]{0,1,2:T(8,128)(2,1)} %reshape.179) | copy-start | bytes 393220
  187.8 2.6 copy-start.3
  191.5 66.2 %reduce-scatter.5.cloned.1.call-start = ((), (), s32[]{:S(2)}) async-start(), calls=%async_computation.8 | async-start | bytes 1769472 | tf_op jit(solution)/shard_map/reduce_scatter | solution.py:203
  225.1 12.3 %all-to-all-start.2 = ((bf16[8,2,4096]{2,1,0:T(2,128)(2,1)}), bf16[8,2,4096]{2,1,0:T(2,128)(2,1)S(1)}, u32[]{:S(2)}, u32[]{:S(2)}) async-start(bf16[8,2,4096]{2,1,0:T(2,128)(2,1)} %reshape.187), calls=%async_computation.3 | async-start | bytes 262144 | tf_op jit(solution)/shard_map/all_to_all | solution.py:189
  236.5 13.7 %copy-start.5 = (bf16[128,2048]{1,0:T(8,128)(2,1)S(1)}, bf16[128,2048]{1,0:T(8,128)(2,1)}, u32[]{:S(2)}) copy-start(bf16[128,2048]{1,0:T(8,128)(2,1)} %param.12) | copy-start | bytes 1572868
  236.5 13.7 %copy-start.12 = (f32[2048]{0:T(1024)S(1)}, f32[2048]{0:T(1024)}, u32[]{:S(2)}) copy-start(f32[2048]{0:T(1024)} %param.14) | copy-start | bytes 24580
  237.4 9.7 %all-to-all-start.3 = ((bf16[8,2,4096]{2,1,0:T(2,128)(2,1)}), bf16[8,2,4096]{2,1,0:T(2,128)(2,1)S(1)}, u32[]{:S(2)}, u32[]{:S(2)}) async-start(bf16[8,2,4096]{2,1,0:T(2,128)(2,1)} %reshape.189), calls=%async_computation.4 | async-start | bytes 262144 | tf_op jit(solution)/shard_map/all_to_all | solution.py:190
  241.6 105.1 %all-reduce.2.cloned.1.call-start = ((), (), s32[]{:S(2)}) async-start(), calls=%async_computation.9 | async-start | bytes 4194304 | tf_op jit(solution)/shard_map/psum | solution.py:213
  243.4 9.4 %copy-start.14 = (f32[128]{0:T(128)S(1)}, f32[128]{0:T(128)}, u32[]{:S(2)}) copy-start(f32[128]{0:T(128)} %get-tuple-element.135) | copy-start | bytes 1540
  243.4 9.4 %copy-start.16 = (f32[128]{0:T(128)S(1)}, f32[128]{0:T(128)}, u32[]{:S(2)}) copy-start(f32[128]{0:T(128)} %copy-done.15) | copy-start | bytes 1540
  244.1 13.6 %copy-start.6 = (bf16[24,2048]{1,0:T(8,128)(2,1)S(1)}, bf16[24,2048]{1,0:T(8,128)(2,1)}, u32[]{:S(2)}) copy-start(bf16[24,2048]{1,0:T(8,128)(2,1)} %param.11) | copy-start | bytes 294916
  244.1 13.6 %copy-start.10 = (f32[2048]{0:T(1024)S(1)}, f32[2048]{0:T(1024)}, u32[]{:S(2)}) copy-start(f32[2048]{0:T(1024)} %param.13) | copy-start | bytes 24580
  247.4 11.4 %copy-start.9 = (bf16[24,2048]{1,0:T(8,128)(2,1)S(1)}, bf16[24,2048]{1,0:T(8,128)(2,1)}, u32[]{:S(2)}) copy-start(bf16[24,2048]{1,0:T(8,128)(2,1)} %param.19) | copy-start | bytes 294916
  247.4 11.4 %copy-start.13 = (f32[24]{0:T(128)S(1)}, f32[24]{0:T(128)}, u32[]{:S(2)}) copy-start(f32[24]{0:T(128)} %get-tuple-element.137) | copy-start | bytes 292
Sparse Core Ops, SparseCore 0:
  9.9 30.4 all-gather.4
  42.3 28.7 all-gather.6
  191.7 23.5 reduce-scatter.6
  218.4 39.2 reduce-scatter.4
  260.5 86.1 all-reduce.1
where the time goes:
time: 358 us; the launch traced here: 356 us
  waiting for transfers between devices  130 us (36%)
  blocking collectives  114 us (32%)
  matrix products  51.2 us (14%)
  local copies, waits for them, and re-layouts  18.9 us (5%)
  starting transfers between devices  14.7 us (4%)
  between operations  14.2 us (4%)
  other arithmetic  12.3 us (3%)
    psum x1, waiting for transfers between devices, body(): out_weight_grad = lax.psum(weight_part, 'sp')  86.2 us
    unnamed x6, waiting for transfers between devices  25.1 us
    all_gather x2, blocking collectives, body(): pieces = lax.all_gather((normed_t, out_cotangent), 'tp', axis=0, tiled=True)  23.6 us
    all_gather x1, blocking collectives, body(): lax.all_gather(key_flat, 'sp', axis=0, tiled=True)  16.4 us
    all_gather x1, blocking collectives, body(): lax.all_gather(value_flat, 'sp', axis=0, tiled=True)  16 us
    all_gather x1, blocking collectives, body(): lax.all_gather(d_attended, 'sp', axis=0, tiled=True)  15.1 us
    all_gather x1, blocking collectives, body(): lax.all_gather(queries, 'sp', axis=0, tiled=True)  15 us
    all_gather x1, blocking collectives, body(): lax.all_gather(log_total, 'sp', axis=0, tiled=True)  14.5 us
  transfers between devices with their start and end apart: 9, of which 5 were waited for; matrix products, arithmetic and copies ran while one was open for 11% of the time, Pallas kernels for 0%

commit v1 on v0

--- a/solution.py
+++ b/solution.py
@@ -7,6 +7,15 @@
 KV_HEADS = 8
 EPSILON = 1e-06
 NEGATIVE = -1e30
+
+
+def add_in_pairs(x, name):
+    size = lax.axis_size(name)
+    summed, reach = (x, 1)
+    while reach < size:
+        summed = summed + lax.ppermute(summed, name, [(i, i ^ reach) for i in range(size)])
+        reach = 2 * reach
+    return summed
 
 
 def normalize(matrix, gain_vector):
@@ -210,7 +219,7 @@
         target_rows, target_gain, d_normed_t
     )
     weight_part = jnp.dot(attended.T, cotangent_block, preferred_element_type=jnp.float32)
-    out_weight_grad = lax.psum(weight_part, "sp")
+    out_weight_grad = add_in_pairs(weight_part, "sp")
     return (target_grad, source_grad, out_weight_grad)
 
 

time: 358 us -> 373 us (1.042)
  other arithmetic: 12.3 us -> 19.8 us
  waiting for transfers between devices: 130 us -> 134 us
    psum x1 -> x0, waiting for transfers between devices: 86.2 us -> none  [body(): out_weight_grad = lax.psum(weight_part, 'sp')]
    ppermute x0 -> x2, waiting for transfers between devices: none -> 84.4 us  [add_in_pairs(): lax.ppermute(summed, name, [(i, i ^ reach) for i in range(size)])]
    unnamed x6 -> x5, waiting for transfers between devices: 25.1 us -> 34 us
    add x0 -> x2, other arithmetic: none -> 5.83 us  [add_in_pairs(): summed + lax.ppermute(summed, name, [(i, i ^ reach) for i in range(size)])]
    unnamed x45 -> x56, local copies, waits for them, and re-layouts: 10.9 us -> 11.6 us
  transfers between devices with their start and end apart: 9 -> 10, of which waited for: 5 -> 4; matrix products, arithmetic and copies ran while one was open for 11% -> 14% of each run, Pallas kernels for 0% -> 0%
where the time goes in v1:
time: 373 us; the launch traced here: 371 us
  waiting for transfers between devices  134 us (36%)
  blocking collectives  114 us (31%)
  matrix products  49.6 us (13%)
  local copies, waits for them, and re-layouts  21.2 us (6%)
  other arithmetic  19.8 us (5%)
  starting transfers between devices  17.7 us (5%)
  between operations  14.3 us (4%)
    ppermute x2, waiting for transfers between devices, add_in_pairs(): lax.ppermute(summed, name, [(i, i ^ reach) for i in range(size)])  84.4 us
    unnamed x5, waiting for transfers between devices  34 us
    all_gather x2, blocking collectives, body(): pieces = lax.all_gather((normed_t, out_cotangent), 'tp', axis=0, tiled=True)  23.7 us
    all_gather x1, blocking collectives, body(): lax.all_gather(key_flat, 'sp', axis=0, tiled=True)  16.3 us
    all_gather x1, blocking collectives, body(): lax.all_gather(value_flat, 'sp', axis=0, tiled=True)  16 us
    all_gather x1, blocking collectives, body(): lax.all_gather(d_attended, 'sp', axis=0, tiled=True)  15.1 us
    all_gather x1, blocking collectives, body(): lax.all_gather(queries, 'sp', axis=0, tiled=True)  15 us
    all_gather x1, blocking collectives, body(): lax.all_gather(log_total, 'sp', axis=0, tiled=True)  14.6 us
  transfers between devices with their start and end apart: 10, of which 4 were waited for; matrix products, arithmetic and copies ran while one was open for 14% of the time, Pallas kernels for 0%

profile of v1, /device:TPU:0, one launch (start us, length us, event | category | flops | bytes accessed | tf_op | source)
XLA Modules:
  0.0 371.3 jit_solution(3008800122920127305)
XLA Ops:
  8.0 0.7 all-gather.7.cloned.1.call-update
  8.7 1.0 fusion.42
  10.3 1.0 fusion.44
  11.3 11.9 %all_gather.31 = bf16[192,2048]{1,0:T(8,128)(2,1)S(1)} all-gather(bf16[24,2048]{1,0:T(8,128)(2,1)S(1)} %fusion.44), channel_id=1, replica_groups=mesh['sp'=4,'tp'=8] {'tp'}, dimensions={0}, use_global_device_ids=true | all-gather | bytes 884736 | tf_op jit(solution)/shard_map/all_gather | solution.py:80
  23.6 0.8 copy.77
  24.4 15.0 %all_gather.32 = bf16[768,256]{1,0:T(8,128)(2,1)S(1)} all-gather(bf16[192,256]{1,0:T(8,128)(2,1)S(1)} %convolution_convert_fusion.3), channel_id=1, replica_groups=mesh['sp'=4,'tp'=8] {'sp'}, dimensions={0}, use_global_device_ids=true | all-gather | bytes 491520 | tf_op jit(solution)/shard_map/all_gather | solution.py:141
  39.5 1.2 fusion.36
  40.8 11.8 %all_gather.37 = bf16[192,2048]{1,0:T(8,128)(2,1)S(1)} all-gather(bf16[24,2048]{1,0:T(8,128)(2,1)} %param.19), channel_id=1, replica_groups=mesh['sp'=4,'tp'=8] {'tp'}, dimensions={0}, use_global_device_ids=true | all-gather | bytes 884736 | tf_op jit(solution)/shard_map/all_gather | solution.py:80
  53.2 2.1 convolution_convert_fusion.1
  55.3 0.8 copy.74
  56.1 3.4 all-to-all-start
  59.5 11.9 %all-gather.7.cloned.1.call-done = bf16[2048,512]{1,0:T(8,128)(2,1)} async-done(((bf16[256,512]{1,0:T(8,128)(2,1)}), bf16[2048,512]{1,0:T(8,128)(2,1)}) %all-gather.7.cloned.1.call-update) | async-done | bytes 2097168 | tf_op jit(solution)/shard_map/all_gather | solution.py:61
  71.3 2.1 convolution_convert_fusion
  73.4 0.7 copy.78
  74.2 3.4 all-to-all-start.1
  77.7 0.7 reshape.179
  78.4 16.3 %all_gather.33 = bf16[4096,64]{0,1:T(8,128)(2,1)S(1)} all-gather(bf16[1024,64]{0,1:T(8,128)(2,1)S(1)} %bitcast.239), channel_id=1, replica_groups=mesh['sp'=4,'tp'=8] {'sp'}, dimensions={0}, use_global_device_ids=true | all-gather | bytes 655360 | tf_op jit(solution)/shard_map/all_gather | solution.py:97
  94.8 0.7 reshape.180
  95.5 16.0 %all_gather.35 = bf16[4096,64]{0,1:T(8,128)(2,1)S(1)} all-gather(bf16[1024,64]{0,1:T(8,128)(2,1)S(1)} %bitcast.240), channel_id=1, replica_groups=mesh['sp'=4,'tp'=8] {'sp'}, dimensions={0}, use_global_device_ids=true | all-gather | bytes 655360 | tf_op jit(solution)/shard_map/all_gather | solution.py:98
  111.5 23.2 %while.3 = (s32[]{:T(128)}, f32[1,4,192]{2,1,0:T(4,128)S(1)}, f32[1,4,192]{2,1,0:T(4,128)S(1)}, f32[1,4,192,64]{2,3,1,0:T(8,128)S(1)}, s32[2]{0:T(128)S(1)}, /*i...) while((s32[]{:T(128)}, f32[1,4,192]{2,1,0:T(4,128)S(1)}, ...), condition=%wide.region_5.6_spmd.clone, body=%wide.region_2.5_spmd.clone.sunk | while | flops 415388160 | bytes 45173076 | solution.py:125
  112.7 4.6 %bitcast_reduce_fusion.3 = (f32[4,192]{1,0:T(4,128)S(1)}, f32[2048,192,4]{0,1,2:T(8,128)}) fusion(bf16[192,1,4,64]{0,3,2,1:T(8,128)(2,1)} %get-tuple-element.230, bf16[4096,64]{0,1:T(8,128)(2,1)S(1)} %get-tuple-element.229, s32[]{:T(128)S(6)} %select_n.6), kind=kOutput, calls=%fused_computation.1.clone.1 | convolution fusion | flops 204471552 | bytes 6654980 | tf_op jit(solution)/shard_map/while/body/eval_jaxpr/tgqd,sgd->gqts/dot_general | solution.py:110
  117.3 4.3 %fusion.90 = f32[1,4,192,64]{2,3,1,0:T(8,128)S(1)} fusion(f32[2048,192,4]{0,1,2:T(8,128)} %get-tuple-element.198, f32[4,192]{1,0:T(4,128)S(1)} %bitcast.230, f32[1,4,192,64]{2,3,1,0:T(8,128)S(1)} %get-tuple-element.215, bf16[4096,64]{0,1:T(8,128)(2,1)S(1)} %get-tuple-element.231, s32[]{:T(128)S(6)} %select_n.6, f32[4,192]{1,0:T(4,128)S(1)} %get-tuple-element.199, ...), kind=kOutput, calls=%fused_computation.8.clone.1 | convolution fusion | flops 206192640 | bytes 7020549 | tf_op jit(solution)/shard_map/while/body/eval_jaxpr/gqts,sgd->gqtd/dot_general | solution.py:117
  121.9 1.2 fusion.89
  124.3 4.6 %bitcast_reduce_fusion.3 = (f32[4,192]{1,0:T(4,128)S(1)}, f32[2048,192,4]{0,1,2:T(8,128)}) fusion(bf16[192,1,4,64]{0,3,2,1:T(8,128)(2,1)} %get-tuple-element.230, bf16[4096,64]{0,1:T(8,128)(2,1)S(1)} %get-tuple-element.229, s32[]{:T(128)S(6)} %select_n.6), kind=kOutput, calls=%fused_computation.1.clone.1 | convolution fusion | flops 204471552 | bytes 6654980 | tf_op jit(solution)/shard_map/while/body/eval_jaxpr/tgqd,sgd->gqts/dot_general | solution.py:110
  128.9 4.3 %fusion.90 = f32[1,4,192,64]{2,3,1,0:T(8,128)S(1)} fusion(f32[2048,192,4]{0,1,2:T(8,128)} %get-tuple-element.198, f32[4,192]{1,0:T(4,128)S(1)} %bitcast.230, f32[1,4,192,64]{2,3,1,0:T(8,128)S(1)} %get-tuple-element.215, bf16[4096,64]{0,1:T(8,128)(2,1)S(1)} %get-tuple-element.231, s32[]{:T(128)S(6)} %select_n.6, f32[4,192]{1,0:T(4,128)S(1)} %get-tuple-element.199, ...), kind=kOutput, calls=%fused_computation.8.clone.1 | convolution fusion | flops 206192640 | bytes 7020549 | tf_op jit(solution)/shard_map/while/body/eval_jaxpr/gqts,sgd->gqtd/dot_general | solution.py:117
  133.5 1.2 fusion.89
  134.9 1.7 convert_multiply_fusion.8
  136.6 15.1 %all_gather.38 = bf16[768,256]{1,0:T(8,128)(2,1)S(1)} all-gather(bf16[192,256]{1,0:T(8,128)(2,1)S(1)} %get-tuple-element.140), channel_id=1, replica_groups=mesh['sp'=4,'tp'=8] {'sp'}, dimensions={0}, use_global_device_ids=true | all-gather | bytes 491520 | tf_op jit(solution)/shard_map/all_gather | solution.py:142
  152.1 13.2 %all-gather.1 = f32[4,192,4]{1,2,0:T(4,128)S(1)} all-gather(f32[1,192,4]{1,2,0:T(4,128)S(1)} %bitcast.250), channel_id=1, replica_groups=mesh['sp'=4,'tp'=8] {'sp'}, dimensions={0}, use_global_device_ids=true | all-gather | bytes 15360 | tf_op jit(solution)/shard_map/all_gather | solution.py:146
  165.6 14.6 %all-gather = f32[768,1,4]{2,1,0:T(1,128)S(1)} all-gather(f32[192,1,4]{2,1,0:T(1,128)S(1)} %bitcast.247), channel_id=2, replica_groups=mesh['sp'=4,'tp'=8] {'sp'}, dimensions={0}, use_global_device_ids=true | all-gather | bytes 15360 | tf_op jit(solution)/shard_map/all_gather | solution.py:145
  180.3 2.8 fusion.54
  183.1 3.2 fusion.27
  186.3 1.3 copy-done.2
  187.6 1.2 convolution_multiply_fusion
  188.9 1.4 copy-done.3
  190.2 1.1 copy.98
  191.5 1.6 fusion.56
  193.1 1.4 collective-permute-start
  194.5 32.6 %reduce-scatter.7.cloned.1.call-done = f32[192,256]{1,0:T(8,128)} async-done(((f32[768,256]{1,0:T(8,128)}), f32[192,256]{1,0:T(8,128)}) %reduce-scatter.7.cloned.1.call-update) | async-done | bytes 196624
  227.1 1.7 copy.99
  228.8 2.6 fusion.57
  231.4 5.4 %fusion.35 = bf16[1024,1,64]{0,2,1:T(8,128)(2,1)} fusion(bf16[768,4,64]{0,2,1:T(8,128)(2,1)S(1)} %bitcast.225, bf16[4,768,1024]{1,2,0:T(8,128)(2,1)} %copy-done.3), kind=kOutput, calls=%fused_computation.43 | convolution fusion | flops 402784256 | bytes 6815744 | tf_op jit(solution)/shard_map/while/body/eval_jaxpr/gqts,tgqd->sgd/dot_general | solution.py:182
  237.4 1.6 reduce.2
  239.1 0.9 reshape.187
  240.0 3.7 all-to-all-start.2
  243.7 7.0 %fusion.31 = bf16[1024,1,64]{0,2,1:T(8,128)(2,1)S(1)} fusion(bf16[768,4,64]{0,2,1:T(8,128)(2,1)} %bitcast.228, f32[1024,768,4]{1,0,2:T(8,128)} %copy-done.2, f32[4,768]{1,0:T(4,128)S(1)} %copy.81), kind=kOutput, calls=%fused_computation.40 | convolution fusion | flops 412090368 | bytes 13119488 | tf_op jit(solution)/shard_map/while/body/eval_jaxpr/gqts,tgqd->sgd/dot_general | solution.py:164
  250.7 1.3 reduce.3
  252.0 1.1 copy.109
  253.1 0.9 reshape.189
  253.9 4.2 %all-to-all-start.3 = ((bf16[8,2,4096]{2,1,0:T(2,128)(2,1)}), bf16[8,2,4096]{2,1,0:T(2,128)(2,1)}, u32[]{:S(2)}, u32[]{:S(2)}) async-start(bf16[8,2,4096]{2,1,0:T(2,128)(2,1)} %reshape.189), calls=%async_computation.4 | async-start | bytes 262144 | tf_op jit(solution)/shard_map/all_to_all | solution.py:199
  258.2 1.0 reshape.188
  259.2 1.2 copy.89
  260.4 3.3 all-to-all-done.3
  263.8 1.8 reshape.190
  265.6 1.2 copy.93
  266.9 2.7 add.67
  269.7 1.6 collective-permute-start.1
  271.2 0.8 fusion.55
  272.1 0.9 fusion.41
  273.0 1.3 fusion.40
  274.4 1.1 fusion.48
  275.5 1.7 fusion.47
  277.2 84.4 %collective-permute-done.1 = f32[256,2048]{1,0:T(8,128)} collective-permute-done((f32[256,2048]{1,0:T(8,128)S(1)}, f32[256,2048]{1,0:T(8,128)}, u32[]{:S(2)}, u32[]{:S(2)}) %collective-permute-start.1) | collective-permute-done | bytes 2097184 | tf_op jit(solution)/shard_map/ppermute | solution.py:16
  361.6 3.2 add.68
  (105 shorter events, 6.5 us)
Async XLA Ops:
  7.2 16.1 %copy-start = (bf16[2048,256]{1,0:T(8,128)(2,1)S(1)}, bf16[2048,256]{1,0:T(8,128)(2,1)}, u32[]{:S(2)}) copy-start(bf16[2048,256]{1,0:T(8,128)(2,1)} %param.15) | copy-start | bytes 3145732
  7.2 46.0 %copy-start.6 = (bf16[128,2048]{1,0:T(8,128)(2,1)S(1)}, bf16[128,2048]{1,0:T(8,128)(2,1)}, u32[]{:S(2)}) copy-start(bf16[128,2048]{1,0:T(8,128)(2,1)} %param.12) | copy-start | bytes 1572868
  7.2 46.0 %copy-start.17 = (f32[2048]{0:T(1024)S(1)}, f32[2048]{0:T(1024)}, u32[]{:S(2)}) copy-start(f32[2048]{0:T(1024)} %param.14) | copy-start | bytes 24580
  7.2 46.0 %all-gather.5.cloned.1.call-start = ((), (), s32[]{:S(2)}) async-start(), calls=%async_computation.6 | async-start | bytes 2359296 | tf_op jit(solution)/shard_map/all_gather | solution.py:60
  7.9 63.4 %all-gather.7.cloned.1.call-start = ((), (), s32[]{:S(2)}) async-start(), calls=%async_computation.7 | async-start | bytes 2359296 | tf_op jit(solution)/shard_map/all_gather | solution.py:61
  52.6 82.3 %copy-start.5 = (bf16[192,2048]{1,0:T(8,128)(2,1)}, bf16[192,2048]{1,0:T(8,128)(2,1)S(1)}, u32[]{:S(2)}) copy-start(bf16[192,2048]{1,0:T(8,128)(2,1)S(1)} %all_gather.37) | copy-start | bytes 2359300
  53.2 42.3 %copy-start.21 = (f32[128]{0:T(128)}, f32[128]{0:T(128)S(1)}, u32[]{:S(2)}) copy-start(f32[128]{0:T(128)S(1)} %get-tuple-element.136) | copy-start | bytes 1540
  56.1 18.1 %all-to-all-start = ((bf16[128,8,64]{0,2,1:T(8,128)(2,1)}), bf16[128,8,64]{0,2,1:T(8,128)(2,1)S(1)}, u32[]{:S(2)}, u32[]{:S(2)}) async-start(bf16[128,8,64]{0,2,1:T(8,128)(2,1)} %bitcast), calls=%async_computation | async-start | bytes 262144 | tf_op jit(solution)/shard_map/all_to_all | solution.py:74
  74.2 20.5 %all-to-all-start.1 = ((bf16[128,8,64]{0,2,1:T(8,128)(2,1)}), bf16[128,8,64]{0,2,1:T(8,128)(2,1)S(1)}, u32[]{:S(2)}, u32[]{:S(2)}) async-start(bf16[128,8,64]{0,2,1:T(8,128)(2,1)} %bitcast.7), calls=%async_computation.1 | async-start | bytes 262144 | tf_op jit(solution)/shard_map/all_to_all | solution.py:75
  77.6 149.5 %reduce-scatter.7.cloned.1.call-start = ((), (), s32[]{:S(2)}) async-start(), calls=%async_computation.9 | async-start | bytes 983040
  111.5 1.2 copy-start.23
  117.3 4.6 %copy-start.1 = (f32[2048,192,4]{0,1,2:T(8,128)S(1)}, f32[2048,192,4]{0,1,2:T(8,128)}, u32[]{:S(2)}) copy-start(f32[2048,192,4]{0,1,2:T(8,128)} %get-tuple-element.198) | copy-start | bytes 18874372 | tf_op jit(solution)/shard_map/while
  117.3 5.8 %copy-start.24 = (s32[2]{0:T(128)S(1)}, s32[2]{0:T(128)}, u32[]{:S(2)}) copy-start(s32[2]{0:T(128)} %copy-done.23) | copy-start | bytes 28 | tf_op jit(solution)/shard_map/while
  123.1 1.2 copy-start.23
  128.9 4.6 %copy-start.1 = (f32[2048,192,4]{0,1,2:T(8,128)S(1)}, f32[2048,192,4]{0,1,2:T(8,128)}, u32[]{:S(2)}) copy-start(f32[2048,192,4]{0,1,2:T(8,128)} %get-tuple-element.198) | copy-start | bytes 18874372 | tf_op jit(solution)/shard_map/while
  128.9 5.8 %copy-start.24 = (s32[2]{0:T(128)S(1)}, s32[2]{0:T(128)}, u32[]{:S(2)}) copy-start(s32[2]{0:T(128)} %copy-done.23) | copy-start | bytes 28 | tf_op jit(solution)/shard_map/while
  134.8 48.3 %copy-start.13 = (bf16[1,4,192,64]{2,3,1,0:T(8,128)(2,1)}, bf16[1,4,192,64]{2,3,1,0:T(8,128)(2,1)S(1)}, u32[]{:S(2)}) copy-start(bf16[1,4,192,64]{2,3,1,0:T(8,128)(2,1)S(1)} %divide_convert_fusion) | copy-start | bytes 294916
  151.9 31.2 %copy-start.8 = (bf16[768,256]{0,1:T(8,128)(2,1)}, bf16[768,256]{0,1:T(8,128)(2,1)S(1)}, u32[]{:S(2)}) copy-start(bf16[768,256]{0,1:T(8,128)(2,1)S(1)} %copy.82) | copy-start | bytes 1179652
  180.3 2.8 copy-start.14
  183.1 4.5 %copy-start.2 = (f32[1024,768,4]{1,0,2:T(8,128)}, f32[1024,768,4]{1,0,2:T(8,128)S(1)}, u32[]{:S(2)}) copy-start(f32[1024,768,4]{1,0,2:T(8,128)S(1)} %fusion.54) | copy-start | bytes 37748740
  183.1 4.5 %copy-start.12 = (bf16[1024,64,1]{0,1,2:T(8,128)(2,1)S(1)}, bf16[1024,64,1]{0,1,2:T(8,128)(2,1)}, u32[]{:S(2)}) copy-start(bf16[1024,64,1]{0,1,2:T(8,128)(2,1)} %reshape.179) | copy-start | bytes 393220
  187.6 2.6 copy-start.3
  191.4 83.0 %reduce-scatter.5.cloned.1.call-start = ((), (), s32[]{:S(2)}) async-start(), calls=%async_computation.8 | async-start | bytes 1769472 | tf_op jit(solution)/shard_map/reduce_scatter | solution.py:212
  193.1 46.9 %copy-start.4 = (f32[256,2048]{1,0:T(8,128)}, f32[256,2048]{1,0:T(8,128)S(1)}, u32[]{:S(2)}) copy-start(f32[256,2048]{1,0:T(8,128)S(1)} %fusion.56) | copy-start | bytes 6291460
  193.1 73.8 %collective-permute-start = (f32[256,2048]{1,0:T(8,128)S(1)}, f32[256,2048]{1,0:T(8,128)}, u32[]{:S(2)}, u32[]{:S(2)}) collective-permute-start(f32[256,2048]{1,0:T(8,128)S(1)} %fusion.56), channel_id=1, source_target_pairs={{0,8},{8,0},{16,24},{24,16},{1,9},{9,1},{17,25},{25,17},{2,10},{10... | collective-permute-start | bytes 6291464 | tf_op jit(solution)/shard_map/ppermute | solution.py:16
  240.0 13.9 %all-to-all-start.2 = ((bf16[8,2,4096]{2,1,0:T(2,128)(2,1)}), bf16[8,2,4096]{2,1,0:T(2,128)(2,1)S(1)}, u32[]{:S(2)}, u32[]{:S(2)}) async-start(bf16[8,2,4096]{2,1,0:T(2,128)(2,1)} %reshape.187), calls=%async_computation.3 | async-start | bytes 262144 | tf_op jit(solution)/shard_map/all_to_all | solution.py:198
  253.9 9.8 %all-to-all-start.3 = ((bf16[8,2,4096]{2,1,0:T(2,128)(2,1)}), bf16[8,2,4096]{2,1,0:T(2,128)(2,1)}, u32[]{:S(2)}, u32[]{:S(2)}) async-start(bf16[8,2,4096]{2,1,0:T(2,128)(2,1)} %reshape.189), calls=%async_computation.4 | async-start | bytes 262144 | tf_op jit(solution)/shard_map/all_to_all | solution.py:199
  259.2 12.9 %copy-start.18 = (f32[2048]{0:T(1024)S(1)}, f32[2048]{0:T(1024)}, u32[]{:S(2)}) copy-start(f32[2048]{0:T(1024)} %param.14) | copy-start | bytes 24580
  266.8 4.4 %copy-start.10 = (bf16[2048,512]{1,0:T(8,128)(2,1)S(1)}, bf16[2048,512]{1,0:T(8,128)(2,1)}, u32[]{:S(2)}) copy-start(bf16[2048,512]{1,0:T(8,128)(2,1)} %all-gather.5.cloned.1.call-done) | copy-start | bytes 6291460
  266.8 5.3 %copy-start.7 = (bf16[128,2048]{1,0:T(8,128)(2,1)S(1)}, bf16[128,2048]{1,0:T(8,128)(2,1)}, u32[]{:S(2)}) copy-start(bf16[128,2048]{1,0:T(8,128)(2,1)} %param.12) | copy-start | bytes 1572868
  266.8 5.3 %copy-start.9 = (bf16[2048,512]{1,0:T(8,128)(2,1)S(1)}, bf16[2048,512]{1,0:T(8,128)(2,1)}, u32[]{:S(2)}) copy-start(bf16[2048,512]{1,0:T(8,128)(2,1)} %all-gather.7.cloned.1.call-done) | copy-start | bytes 6291460
  266.9 6.1 %copy-start.20 = (f32[128]{0:T(128)S(1)}, f32[128]{0:T(128)}, u32[]{:S(2)}) copy-start(f32[128]{0:T(128)} %get-tuple-element.135) | copy-start | bytes 1540
  266.9 6.1 %copy-start.22 = (f32[128]{0:T(128)S(1)}, f32[128]{0:T(128)}, u32[]{:S(2)}) copy-start(f32[128]{0:T(128)} %copy-done.21) | copy-start | bytes 1540
  269.6 4.8 %copy-start.11 = (bf16[24,2048]{1,0:T(8,128)(2,1)S(1)}, bf16[24,2048]{1,0:T(8,128)(2,1)}, u32[]{:S(2)}) copy-start(bf16[24,2048]{1,0:T(8,128)(2,1)} %param.11) | copy-start | bytes 294916
  269.6 4.8 %copy-start.16 = (f32[2048]{0:T(1024)S(1)}, f32[2048]{0:T(1024)}, u32[]{:S(2)}) copy-start(f32[2048]{0:T(1024)} %param.13) | copy-start | bytes 24580
  269.6 5.8 %copy-start.15 = (bf16[24,2048]{1,0:T(8,128)(2,1)S(1)}, bf16[24,2048]{1,0:T(8,128)(2,1)}, u32[]{:S(2)}) copy-start(bf16[24,2048]{1,0:T(8,128)(2,1)} %param.19) | copy-start | bytes 294916
  269.6 5.8 %copy-start.19 = (f32[24]{0:T(128)S(1)}, f32[24]{0:T(128)}, u32[]{:S(2)}) copy-start(f32[24]{0:T(128)} %get-tuple-element.137) | copy-start | bytes 292
  269.7 92.0 %collective-permute-start.1 = (f32[256,2048]{1,0:T(8,128)S(1)}, f32[256,2048]{1,0:T(8,128)}, u32[]{:S(2)}, u32[]{:S(2)}) collective-permute-start(f32[256,2048]{1,0:T(8,128)S(1)} %add.67), channel_id=1, source_target_pairs={{0,16},{8,24},{16,0},{24,8},{1,17},{9,25},{17,1},{25,9},{2,18},{10... | collective-permute-start | bytes 6291464 | tf_op jit(solution)/shard_map/ppermute | solution.py:16
Sparse Core Ops, SparseCore 0:
  9.9 30.4 all-gather.4
  42.3 28.9 all-gather.6
  191.5 35.5 reduce-scatter.6
  231.6 37.4 reduce-scatter.4
